TPU v7x, 256 devices: a 4x2x16 block of a 4x16x16 slice. The times are simulated.
256 devices in a mesh: grp: 2 (over y), fs: 16 (over z), tp: 8 (over x, core).
Axes of the slice: x: 4, y: 2, z: 16, core: 2. Of those that a mesh axis runs over, the one named last changes fastest.
The devices are a block of a 4x16x16 slice.
Arguments:
- tokens: bfloat16 [128, 128, 2048], P(('grp', 'fs'), None, 'tp'), parts along dimension 0, may hold values from -100 to 100
- mix_gain: float32 [2048], replicated, may hold values from 0.1 to 1.9
- gate_outer: bfloat16 [2048, 1024], P('fs', 'tp'), may hold values from -0.125 to 0.125
- gate_inner: bfloat16 [2048, 1024], P('fs', 'tp'), may hold values from -0.125 to 0.125
- value_weight: bfloat16 [2048, 1024], P('fs', 'tp'), may hold values from -0.125 to 0.125
- conv_taps: float32 [3, 1024], replicated, may hold values from -3 to 3
- mix_out: bfloat16 [1024, 2048], P('tp', 'fs'), may hold values from -0.25 to 0.25
- ffn_gain: float32 [2048], replicated, may hold values from 0.1 to 1.9
- ffn_gate: bfloat16 [2048, 5632], P('fs', 'tp'), may hold values from -0.125 to 0.125
- ffn_up: bfloat16 [2048, 5632], P('fs', 'tp'), may hold values from -0.125 to 0.125
- ffn_down: bfloat16 [5632, 2048], P('tp', 'fs'), may hold values from -0.109375 to 0.109375
- out_gain: float32 [2048], replicated, may hold values from 0.1 to 1.9
Outputs:
- layer_out: bfloat16 [128, 128, 2048], P(('grp', 'fs'), None, 'tp'), parts along dimension 0
There are 2 independent parts, one for each index of `grp`. A program takes and returns all parts, laid end to end along the dimension named above; an argument that names none is the same for every part. Nothing has to cross between parts.
All inputs are finite; a program needn't handle non-finite values.
Results may differ from a plain program's by a relative error of at most 0.015.
Values may be sent and summed in bfloat16 or wider, within the bound.
No kernel may reach another device: no remote copies, remote signals or barrier semaphores. Data moves between devices by JAX's collectives and lax.ppermute only.
A program may use at most 64 MiB of HBM per device.

v0:
```python
import jax
import jax.numpy as jnp
from jax import lax
from jax.sharding import PartitionSpec as P


def in_order(parts, dim):
    parts = jnp.moveaxis(parts, 0, dim)
    shape = parts.shape
    return parts.reshape(*shape[:dim], shape[dim] * shape[dim + 1], *shape[dim + 2 :])


def copy_for_each(shard, axis):
    copies = jnp.broadcast_to(shard, (lax.axis_size(axis), *shard.shape))
    return lax.all_to_all(copies, axis, split_axis=0, concat_axis=0, tiled=True)


def collect(shard, axis, dim):
    return in_order(copy_for_each(shard, axis), dim)


def side_by_side(arrays, axis, dim, along):
    both = jnp.concatenate(arrays, axis=along)
    filled, at, outs = (lax.all_gather(both, axis, axis=dim, tiled=True), 0, [])
    for a in arrays:
        outs.append(lax.slice_in_dim(filled, at, at + a.shape[along], axis=along))
        at += a.shape[along]
    return tuple(outs)


def in_blocks(shard, dim, count):
    shape = shard.shape
    parts = shard.reshape(*shape[:dim], count, shape[dim] // count, *shape[dim + 1 :])
    return jnp.moveaxis(parts, dim, 0)


def summed_on_arrival(shard, axis, dim):
    parts = in_blocks(shard, dim, lax.axis_size(axis))
    arrived = lax.all_to_all(parts, axis, split_axis=0, concat_axis=0, tiled=True)
    return arrived.astype(jnp.float32).sum(axis=0)


def of_everyone(shard, axis):
    return copy_for_each(shard, axis).sum(axis=0)


def rms_norm(values, gain):
    floats = values.astype(jnp.float32)
    scaled = floats * lax.rsqrt(jnp.mean(floats * floats, axis=-1, keepdims=True) + 1e-06)
    return (scaled * gain).astype(jnp.bfloat16)


def local(
    tokens,
    mix_gain,
    gate_outer,
    gate_inner,
    value_weight,
    conv_taps,
    mix_out,
    ffn_gain,
    ffn_gate,
    ffn_up,
    ffn_down,
    out_gain,
):
    seq_count, length, columns = tokens.shape
    row_count = seq_count * length
    width = columns * lax.axis_size("tp")
    whole = collect(tokens, "tp", 2).reshape(row_count, width)
    normed = rms_norm(whole, mix_gain)
    channels = gate_outer.shape[1]
    pieces = side_by_side((gate_outer, gate_inner, value_weight), "fs", 0, 1)
    sliced = normed
    outer = jnp.dot(sliced, pieces[0], preferred_element_type=jnp.float32)
    inner = jnp.dot(sliced, pieces[1], preferred_element_type=jnp.float32)
    values = jnp.dot(sliced, pieces[2], preferred_element_type=jnp.float32)
    outer = outer.astype(jnp.bfloat16)
    inner = inner.astype(jnp.bfloat16)
    values = values.astype(jnp.bfloat16)
    product = (inner.astype(jnp.float32) * values.astype(jnp.float32)).reshape(
        seq_count, length, channels
    )
    own_taps = lax.dynamic_slice_in_dim(conv_taps, lax.axis_index("tp") * channels, channels, 1)
    tap_count = conv_taps.shape[0]
    padded = jnp.pad(product, ((0, 0), (tap_count - 1, 0), (0, 0)))
    conv = jnp.zeros((seq_count, length, channels), jnp.float32)
    for offset in range(tap_count):
        conv = conv + own_taps[offset] * padded[:, offset : offset + length]
    gated = (outer.astype(jnp.float32) * conv.reshape(row_count, channels)).astype(jnp.bfloat16)
    mix_terms = jnp.dot(gated, collect(mix_out, "fs", 1), preferred_element_type=jnp.float32)
    mix_summed = summed_on_arrival(mix_terms.astype(jnp.bfloat16), "tp", 1)
    first = (tokens.reshape(row_count, columns).astype(jnp.float32) + mix_summed).astype(
        jnp.bfloat16
    )
    whole_ffn = collect(first.reshape(seq_count, length, columns), "tp", 2).reshape(
        row_count, width
    )
    normed_ffn = rms_norm(whole_ffn, ffn_gain)
    pieces = side_by_side((ffn_gate, ffn_up), "fs", 0, 1)
    sliced = normed_ffn
    gate = jnp.dot(sliced, pieces[0], preferred_element_type=jnp.float32)
    upward = jnp.dot(sliced, pieces[1], preferred_element_type=jnp.float32)
    hidden = (jax.nn.silu(gate) * upward).astype(jnp.bfloat16)
    down_terms = jnp.dot(
        hidden,
        lax.all_gather(ffn_down, "fs", axis=1, tiled=True),
        preferred_element_type=jnp.float32,
    )
    down_summed = summed_on_arrival(down_terms.astype(jnp.bfloat16), "tp", 1)
    second = first.astype(jnp.float32) + down_summed
    squares = of_everyone(jnp.sum(second * second, axis=1), "tp")
    factor = lax.rsqrt(squares / width + 1e-06)
    own_gain = lax.dynamic_slice_in_dim(out_gain, lax.axis_index("tp") * columns, columns, 0)
    result = second * factor[:, None] * own_gain
    return result.astype(jnp.bfloat16).reshape(seq_count, length, columns)


def solution(mesh):
    in_specs = (
        P(("grp", "fs"), None, "tp"),
        P(),
        P("fs", "tp"),
        P("fs", "tp"),
        P("fs", "tp"),
        P(),
        P("tp", "fs"),
        P(),
        P("fs", "tp"),
        P("fs", "tp"),
        P("tp", "fs"),
        P(),
    )
    out_specs = P(("grp", "fs"), None, "tp")
    return jax.shard_map(local, mesh=mesh, in_specs=in_specs, out_specs=out_specs, check_vma=False)
```

profile of v0, /device:TPU:33, one launch (start us, length us, event | category | flops | bytes accessed | tf_op | source)
XLA Modules:
  0.0 347.9 jit_solution(9210337294262374817)
XLA Ops:
  6.5 0.0 copy-start
  6.6 0.0 all-gather.4.cloned.1.call-start
  6.6 1.5 pad_maximum_fusion.1
  8.0 0.1 all-gather.4.cloned.1.call-update
  8.1 0.1 all-gather.6.cloned.1.call-start
  8.1 1.8 pad_maximum_fusion
  9.9 0.1 all-gather.6.cloned.1.call-update
  10.0 2.5 broadcast_in_dim.20
  12.5 0.0 copy-start.2
  12.5 24.1 %all-to-all-start = ((bf16[8,4,128,256]{3,2,1,0:T(8,128)(2,1)}), bf16[8,4,128,256]{3,2,1,0:T(8,128)(2,1)S(1)}, u32[]{:S(2)}, u32[]{:S(2)}) async-start(bf16[8,4,128,256]{3,2,1,0:T(8,128)(2,1)} %broadcast_in_dim.20), calls=%async_computation | async-start | bytes 4194304 | tf_op jit(solution)/shard_map/all_to_all | solution.py:15
  36.6 0.0 copy-done.2
  36.6 0.1 copy.25
  36.7 0.0 copy-done
  36.7 26.1 %all-to-all-done = bf16[8,4,128,256]{3,2,1,0:T(8,128)(2,1)S(1)} async-done(((bf16[8,4,128,256]{3,2,1,0:T(8,128)(2,1)}), bf16[8,4,128,256]{3,2,1,0:T(8,128)(2,1)S(1)}, u32[]{:S(2)}, u32[]{:S(2)}) %all-to-all-start) | async-done | bytes 2097184 | tf_op jit(solution)/shard_map/all_to_all | solution.py:15
  62.9 0.9 broadcast_in_dim.21
  63.7 5.7 %all-to-all-start.1 = ((bf16[16,128,128]{1,2,0:T(8,128)(2,1)}), bf16[16,128,128]{1,2,0:T(8,128)(2,1)S(1)}, u32[]{:S(2)}, u32[]{:S(2)}) async-start(bf16[16,128,128]{1,2,0:T(8,128)(2,1)} %broadcast_in_dim.21), calls=%async_computation.1 | async-start | bytes 1048576 | tf_op jit(solution)/shard_map/all_to_all | solution.py:15
  69.4 0.5 convert_bitcast_fusion.1
  70.0 2.4 copy.24
  72.4 2.0 copy.33
  74.4 0.0 copy-start.3
  74.4 0.5 fusion
  74.9 0.2 copy-done.3
  75.1 0.4 multiply_convert_fusion.1
  75.5 23.0 %all-gather.4.cloned.1.call-done = bf16[2048,384]{1,0:T(8,128)(2,1)} async-done(((bf16[128,384]{1,0:T(8,128)(2,1)}), bf16[2048,384]{1,0:T(8,128)(2,1)}) %all-gather.4.cloned.1.call-update) | async-done | bytes 1572880 | tf_op jit(solution)/shard_map/all_gather | solution.py:24
  98.4 1.7 fusion.14
  100.2 1.8 fusion.13
  102.0 0.1 fusion.27
  102.0 0.0 all-to-all-done.1
  102.1 4.7 %convolution_convert_fusion = bf16[512,2048]{1,0:T(8,128)(2,1)} fusion(bf16[128,2048]{0,1:T(8,128)(2,1)S(1)} %bitcast.61, f32[512,128]{1,0:T(8,128)S(1)} %bitcast.63, bf16[512,2048]{1,0:T(8,128)(2,1)S(1)} %multiply_convert_fusion.1, bf16[2048,384]{1,0:T(8,128)(2,1)} %all-gather.4.cloned.1.call-done), kind=kOutput, calls=%fused_computation.10 | convolution fusion | flops 538181632 | bytes 5505024 | tf_op jit(solution)/shard_map/dot_general | solution.py:91
  106.7 3.1 copy.38
  109.8 13.0 %all-to-all-start.2 = ((bf16[8,512,256]{2,1,0:T(8,128)(2,1)}), bf16[8,512,256]{2,1,0:T(8,128)(2,1)S(1)}, u32[]{:S(2)}, u32[]{:S(2)}) async-start(bf16[8,512,256]{2,1,0:T(8,128)(2,1)} %bitcast.53), calls=%async_computation.2 | async-start | bytes 4194304 | tf_op jit(solution)/shard_map/all_to_all | solution.py:39
  122.9 0.0 copy-start.1
  122.9 0.0 all-gather.8.cloned.1.call-start
  122.9 0.7 all-gather.8.cloned.1.call-update
  123.6 25.4 %all-to-all-done.2 = bf16[8,512,256]{2,1,0:T(8,128)(2,1)S(1)} async-done(((bf16[8,512,256]{2,1,0:T(8,128)(2,1)}), bf16[8,512,256]{2,1,0:T(8,128)(2,1)S(1)}, u32[]{:S(2)}, u32[]{:S(2)}) %all-to-all-start.2) | async-done | bytes 2097184 | tf_op jit(solution)/shard_map/all_to_all | solution.py:39
  149.1 0.3 convert_reduce_fusion.1
  149.4 0.0 copy-done.1
  149.4 0.1 add_convert_fusion
  149.5 0.2 broadcast_in_dim.22
  149.7 29.7 %all_to_all.31 = bf16[8,4,128,256]{3,2,1,0:T(8,128)(2,1)S(1)} all-to-all(bf16[8,4,128,256]{3,2,1,0:T(8,128)(2,1)S(1)} %broadcast_in_dim.22), channel_id=1, replica_groups=mesh['grp'=2,'fs'=16,'tp'=8] {'tp'}, dimensions={0} | all-to-all | bytes 4194304 | tf_op jit(solution)/shard_map/all_to_all | solution.py:15
  179.4 0.5 convert_bitcast_fusion
  179.9 2.4 copy.27
  182.3 4.0 %copy.34 = f32[64,8,8,256]{3,1,2,0:T(8,128)} copy(f32[64,8,8,256]{3,2,1,0:T(8,128)S(1)} %bitcast.52) | data formatting | bytes 8388608
  186.3 0.0 copy-start.4
  186.3 0.5 fusion.1
  186.8 13.6 %all-gather.6.cloned.1.call-done = bf16[2048,1408]{0,1:T(8,128)(2,1)} async-done(((bf16[128,1408]{0,1:T(8,128)(2,1)}), bf16[2048,1408]{0,1:T(8,128)(2,1)}) %all-gather.6.cloned.1.call-update) | async-done | bytes 5767184 | tf_op jit(solution)/shard_map/all_gather | solution.py:24
  200.4 0.0 copy-done.4
  200.4 6.0 %fusion.4 = f32[512,704]{0,1:T(8,128)} fusion(bf16[2048,1408]{0,1:T(8,128)(2,1)} %all-gather.6.cloned.1.call-done, f32[512,2048]{1,0:T(8,128)} %bitcast.57, f32[2048]{0:T(1024)S(1)} %copy-done.4, f32[512]{0:T(512)S(1)} %rsqrt_bitcast_fusion.1), kind=kOutput, calls=%fused_computation.14 | convolution fusion | flops 1479540736 | bytes 8529920 | tf_op jit(solution)/shard_map/dot_general | solution.py:102
  206.4 74.6 %all-gather.8.cloned.1.call-done = bf16[704,2048]{1,0:T(8,128)(2,1)} async-done(((bf16[704,128]{1,0:T(8,128)(2,1)}), bf16[704,2048]{1,0:T(8,128)(2,1)}) %all-gather.8.cloned.1.call-update) | async-done | bytes 2883600 | tf_op jit(solution)/shard_map/all_gather | solution.py:107
  281.0 7.8 %convolution_convert_fusion.1 = bf16[512,2048]{1,0:T(8,128)(2,1)S(1)} fusion(bf16[704,2048]{1,0:T(8,128)(2,1)} %all-gather.8.cloned.1.call-done, bf16[2048,1408]{0,1:T(8,128)(2,1)} %all-gather.6.cloned.1.call-done, f32[512,704]{0,1:T(8,128)} %fusion.4, f32[512,2048]{1,0:T(8,128)} %bitcast.58, f32[2048]{0:T(1024)S(1)} %copy-done.4, ...), kind=kOutput, calls=%fused_computation.11 | convolution fusion | flops 2959147008 | bytes 13510656 | tf_op jit(solution)/shard_map/dot_general | solution.py:105
  288.9 0.1 copy.37
  289.0 41.4 %all_to_all.32 = bf16[8,512,256]{2,1,0:T(8,128)(2,1)S(1)} all-to-all(bf16[8,512,256]{2,1,0:T(8,128)(2,1)S(1)} %bitcast.55), channel_id=1, replica_groups=mesh['grp'=2,'fs'=16,'tp'=8] {'tp'}, dimensions={0} | all-to-all | bytes 4194304 | tf_op jit(solution)/shard_map/all_to_all | solution.py:39
  330.4 0.3 convert_reduce_fusion
  330.7 0.1 multiply_reduce_fusion
  330.9 0.6 broadcast_in_dim.24
  331.5 4.3 %all-to-all-start.5 = ((f32[8,1,512]{2,1,0:T(1,128)}), f32[8,1,512]{2,1,0:T(1,128)S(1)}, u32[]{:S(2)}, u32[]{:S(2)}) async-start(f32[8,1,512]{2,1,0:T(1,128)} %broadcast_in_dim.24), calls=%async_computation.5 | async-start | bytes 32768 | tf_op jit(solution)/shard_map/all_to_all | solution.py:15
  335.8 0.8 dynamic_slice.7
  336.6 4.0 %all-to-all-done.5 = f32[8,1,512]{2,1,0:T(1,128)S(1)} async-done(((f32[8,1,512]{2,1,0:T(1,128)}), f32[8,1,512]{2,1,0:T(1,128)S(1)}, u32[]{:S(2)}, u32[]{:S(2)}) %all-to-all-start.5) | async-done | bytes 16416 | tf_op jit(solution)/shard_map/all_to_all | solution.py:15
  340.6 0.8 multiply_convert_fusion.2
  (6 shorter events, 0.1 us)
Async XLA Ops:
  6.5 30.1 %copy-start = (f32[3,1024]{1,0:T(4,128)S(1)}, f32[3,1024]{1,0:T(4,128)}, u32[]{:S(2)}) copy-start(f32[3,1024]{1,0:T(4,128)} %param.17) | copy-start | bytes 36868
  6.6 91.9 %all-gather.4.cloned.1.call-start = ((), (), s32[]{:S(2)}) async-start(), calls=%async_computation.6 | async-start | bytes 1671168 | tf_op jit(solution)/shard_map/all_gather | solution.py:24
  8.1 192.4 %all-gather.6.cloned.1.call-start = ((), (), s32[]{:S(2)}) async-start(), calls=%async_computation.7 | async-start | bytes 6127616 | tf_op jit(solution)/shard_map/all_gather | solution.py:24
  12.5 24.1 %copy-start.2 = (bf16[128,128]{1,0:T(8,128)(2,1)S(1)}, bf16[128,128]{1,0:T(8,128)(2,1)}, u32[]{:S(2)}) copy-start(bf16[128,128]{1,0:T(8,128)(2,1)} %param.18) | copy-start | bytes 98308
  12.5 50.4 %all-to-all-start = ((bf16[8,4,128,256]{3,2,1,0:T(8,128)(2,1)}), bf16[8,4,128,256]{3,2,1,0:T(8,128)(2,1)S(1)}, u32[]{:S(2)}, u32[]{:S(2)}) async-start(bf16[8,4,128,256]{3,2,1,0:T(8,128)(2,1)} %broadcast_in_dim.20), calls=%async_computation | async-start | bytes 4194304 | tf_op jit(solution)/shard_map/all_to_all | solution.py:15
  63.7 38.3 %all-to-all-start.1 = ((bf16[16,128,128]{1,2,0:T(8,128)(2,1)}), bf16[16,128,128]{1,2,0:T(8,128)(2,1)S(1)}, u32[]{:S(2)}, u32[]{:S(2)}) async-start(bf16[16,128,128]{1,2,0:T(8,128)(2,1)} %broadcast_in_dim.21), calls=%async_computation.1 | async-start | bytes 1048576 | tf_op jit(solution)/shard_map/all_to_all | solution.py:15
  74.4 0.7 copy-start.3
  109.8 39.2 %all-to-all-start.2 = ((bf16[8,512,256]{2,1,0:T(8,128)(2,1)}), bf16[8,512,256]{2,1,0:T(8,128)(2,1)S(1)}, u32[]{:S(2)}, u32[]{:S(2)}) async-start(bf16[8,512,256]{2,1,0:T(8,128)(2,1)} %bitcast.53), calls=%async_computation.2 | async-start | bytes 4194304 | tf_op jit(solution)/shard_map/all_to_all | solution.py:39
  122.9 26.5 %copy-start.1 = (bf16[4,128,256]{2,1,0:T(8,128)(2,1)S(1)}, bf16[4,128,256]{2,1,0:T(8,128)(2,1)}, u32[]{:S(2)}) copy-start(bf16[4,128,256]{2,1,0:T(8,128)(2,1)} %param.12) | copy-start | bytes 786436
  122.9 158.1 %all-gather.8.cloned.1.call-start = ((), (), s32[]{:S(2)}) async-start(), calls=%async_computation.8 | async-start | bytes 3063808 | tf_op jit(solution)/shard_map/all_gather | solution.py:107
  186.3 14.1 %copy-start.4 = (f32[2048]{0:T(1024)S(1)}, f32[2048]{0:T(1024)}, u32[]{:S(2)}) copy-start(f32[2048]{0:T(1024)} %param.19) | copy-start | bytes 24580
  331.5 9.0 %all-to-all-start.5 = ((f32[8,1,512]{2,1,0:T(1,128)}), f32[8,1,512]{2,1,0:T(1,128)S(1)}, u32[]{:S(2)}, u32[]{:S(2)}) async-start(f32[8,1,512]{2,1,0:T(1,128)} %broadcast_in_dim.24), calls=%async_computation.5 | async-start | bytes 32768 | tf_op jit(solution)/shard_map/all_to_all | solution.py:15
Sparse Core Ops, SparseCore 0:
  9.1 89.2 all-gather.3
  100.2 100.1 all-gather.5
  202.2 78.7 all-gather.7
where the time goes:
time: 349 us; the launch traced here: 348 us
  waiting for transfers between devices  168 us (48%)
  blocking collectives  71.1 us (20%)
  starting transfers between devices  47.1 us (13%)
  matrix products  22 us (6%)
  local copies, waits for them, and re-layouts  19.4 us (6%)
  between operations  13.3 us (4%)
  other arithmetic  7.44 us (2%)
    all_gather x1, waiting for transfers between devices, local(): lax.all_gather(ffn_down, 'fs', axis=1, tiled=True)  74.6 us
    all_to_all x1, blocking collectives, summed_on_arrival(): lax.all_to_all(parts, axis, split_axis=0, concat_axis=0, tiled=True)  41.4 us
    all_gather x2, waiting for transfers between devices, side_by_side(): filled, at, outs = (lax.all_gather(both, axis, axis=dim, tiled=True), 0, [])  36.6 us
    all_to_all x3, starting transfers between devices, copy_for_each(): return lax.all_to_all(copies, axis, split_axis=0, concat_axis=0, tiled=True)  34 us
    all_to_all x3, waiting for transfers between devices, copy_for_each(): return lax.all_to_all(copies, axis, split_axis=0, concat_axis=0, tiled=True)  30.1 us
    all_to_all x1, blocking collectives, copy_for_each(): return lax.all_to_all(copies, axis, split_axis=0, concat_axis=0, tiled=True)  29.7 us
    all_to_all x1, waiting for transfers between devices, summed_on_arrival(): lax.all_to_all(parts, axis, split_axis=0, concat_axis=0, tiled=True)  25.4 us
    all_to_all x1, starting transfers between devices, summed_on_arrival(): lax.all_to_all(parts, axis, split_axis=0, concat_axis=0, tiled=True)  13 us
  transfers between devices with their start and end apart: 7, of which 6 were waited for; matrix products, arithmetic and copies ran while one was open for 11% of the time, Pallas kernels for 0%

commit v1 on v0

--- a/solution.py
+++ b/solution.py
@@ -104,7 +104,9 @@
     hidden = (jax.nn.silu(gate) * upward).astype(jnp.bfloat16)
     down_terms = jnp.dot(
         hidden,
-        lax.all_gather(ffn_down, "fs", axis=1, tiled=True),
+        jnp.concatenate(
+            lax.all_to_all(jnp.stack([ffn_down] * lax.axis_size("fs")), "fs", 0, 0), axis=1
+        ),
         preferred_element_type=jnp.float32,
     )
     down_summed = summed_on_arrival(down_terms.astype(jnp.bfloat16), "tp", 1)

time: 349 us -> 445 us (1.28)
  waiting for transfers between devices: 168 us -> 258 us
    all_gather x2, waiting for transfers between devices: 36.6 us -> 203 us  [side_by_side(): filled, at, outs = (lax.all_gather(both, axis, axis=dim, tiled=True), 0, [])]
    all_gather x1 -> x0, waiting for transfers between devices: 74.6 us -> none  [local(): lax.all_gather(ffn_down, 'fs', axis=1, tiled=True)]
    all_to_all x1 -> x2, blocking collectives: 41.4 us -> 75.4 us  [summed_on_arrival(): lax.all_to_all(parts, axis, split_axis=0, concat_axis=0, tiled=True)]
    all_to_all x1 -> x0, blocking collectives: 29.7 us -> none  [copy_for_each(): return lax.all_to_all(copies, axis, split_axis=0, concat_axis=0, tiled=True)]
    all_to_all x1, waiting for transfers between devices: 25.4 us -> 0.01 us  [local(): lax.all_to_all(jnp.stack([ffn_down] * lax.axis_size('fs')), 'fs', 0, 0)]
    all_to_all x3 -> x4, waiting for transfers between devices: 30.1 us -> 54.8 us  [copy_for_each(): return lax.all_to_all(copies, axis, split_axis=0, concat_axis=0, tiled=True)]
    all_to_all x1, starting transfers between devices: 13 us -> 8.13 us  [local(): lax.all_to_all(jnp.stack([ffn_down] * lax.axis_size('fs')), 'fs', 0, 0)]
    all_to_all x3 -> x4, starting transfers between devices: 34 us -> 38.7 us  [copy_for_each(): return lax.all_to_all(copies, axis, split_axis=0, concat_axis=0, tiled=True)]
  transfers between devices with their start and end apart: 7 -> 7, of which waited for: 6 -> 5; matrix products, arithmetic and copies ran while one was open for 11% -> 6% of each run, Pallas kernels for 0% -> 0%
where the time goes in v1:
time: 445 us; the launch traced here: 444 us
  waiting for transfers between devices  258 us (58%)
  blocking collectives  75.4 us (17%)
  starting transfers between devices  46.9 us (11%)
  local copies, waits for them, and re-layouts  22.1 us (5%)
  matrix products  22 us (5%)
  between operations  13.7 us (3%)
  other arithmetic  5.61 us (1%)
    all_gather x2, waiting for transfers between devices, side_by_side(): filled, at, outs = (lax.all_gather(both, axis, axis=dim, tiled=True), 0, [])  203 us
    all_to_all x2, blocking collectives, summed_on_arrival(): lax.all_to_all(parts, axis, split_axis=0, concat_axis=0, tiled=True)  75.4 us
    all_to_all x4, waiting for transfers between devices, copy_for_each(): return lax.all_to_all(copies, axis, split_axis=0, concat_axis=0, tiled=True)  54.8 us
    all_to_all x4, starting transfers between devices, copy_for_each(): return lax.all_to_all(copies, axis, split_axis=0, concat_axis=0, tiled=True)  38.7 us
  transfers between devices with their start and end apart: 7, of which 5 were waited for; matrix products, arithmetic and copies ran while one was open for 6% of the time, Pallas kernels for 0%

profile of v1, /device:TPU:33, one launch (start us, length us, event | category | flops | bytes accessed | tf_op | source)
XLA Modules:
  0.0 443.9 jit_solution(6071463160645724557)
XLA Ops:
  6.5 0.0 copy-start
  6.6 2.5 broadcast_in_dim.20
  9.1 24.1 %all-to-all-start = ((bf16[8,4,128,256]{3,2,1,0:T(8,128)(2,1)}), bf16[8,4,128,256]{3,2,1,0:T(8,128)(2,1)S(1)}, u32[]{:S(2)}, u32[]{:S(2)}) async-start(bf16[8,4,128,256]{3,2,1,0:T(8,128)(2,1)} %broadcast_in_dim.20), calls=%async_computation | async-start | bytes 4194304 | tf_op jit(solution)/shard_map/all_to_all | solution.py:15
  33.2 0.0 all-gather.3.cloned.1.call-start
  33.2 0.0 copy-done.7
  33.2 0.0 copy-done.8
  33.2 0.0 copy-done.9
  33.2 0.7 pad_maximum_fusion.1
  33.8 0.1 all-gather.3.cloned.1.call-update
  33.9 0.0 copy-done.6
  33.9 0.1 copy.27
  34.1 0.0 copy-done
  34.1 25.4 %all-to-all-done = bf16[8,4,128,256]{3,2,1,0:T(8,128)(2,1)S(1)} async-done(((bf16[8,4,128,256]{3,2,1,0:T(8,128)(2,1)}), bf16[8,4,128,256]{3,2,1,0:T(8,128)(2,1)S(1)}, u32[]{:S(2)}, u32[]{:S(2)}) %all-to-all-start) | async-done | bytes 2097184 | tf_op jit(solution)/shard_map/all_to_all | solution.py:15
  59.5 0.9 broadcast_in_dim.21
  60.4 5.7 %all-to-all-start.1 = ((bf16[16,128,128]{1,2,0:T(8,128)(2,1)}), bf16[16,128,128]{1,2,0:T(8,128)(2,1)S(1)}, u32[]{:S(2)}, u32[]{:S(2)}) async-start(bf16[16,128,128]{1,2,0:T(8,128)(2,1)} %broadcast_in_dim.21), calls=%async_computation.1 | async-start | bytes 1048576 | tf_op jit(solution)/shard_map/all_to_all | solution.py:15
  66.0 0.5 convert_bitcast_fusion.1
  66.6 2.4 copy.26
  69.0 2.0 copy.37
  71.0 0.0 copy-start.10
  71.0 0.5 fusion
  71.5 0.2 copy-done.10
  71.7 0.4 multiply_convert_fusion.1
  72.1 35.0 %all-gather.3.cloned.1.call-done = bf16[2048,384]{1,0:T(8,128)(2,1)} async-done(((bf16[128,384]{1,0:T(8,128)(2,1)}), bf16[2048,384]{1,0:T(8,128)(2,1)}) %all-gather.3.cloned.1.call-update) | async-done | bytes 1572880 | tf_op jit(solution)/shard_map/all_gather | solution.py:24
  107.1 1.7 fusion.16
  108.8 1.8 fusion.15
  110.6 0.1 fusion.29
  110.7 0.0 all-to-all-done.1
  110.7 4.7 %convolution_convert_fusion = bf16[512,2048]{1,0:T(8,128)(2,1)} fusion(bf16[128,2048]{0,1:T(8,128)(2,1)S(1)} %bitcast.68, f32[512,128]{1,0:T(8,128)S(1)} %bitcast.70, bf16[512,2048]{1,0:T(8,128)(2,1)S(1)} %multiply_convert_fusion.1, bf16[2048,384]{1,0:T(8,128)(2,1)} %all-gather.3.cloned.1.call-done), kind=kOutput, calls=%fused_computation.10 | convolution fusion | flops 538181632 | bytes 5505024 | tf_op jit(solution)/shard_map/dot_general | solution.py:91
  115.4 1.7 copy.46
  117.1 37.0 %all_to_all.36 = bf16[8,512,256]{2,1,0:T(8,128)(2,1)S(1)} all-to-all(bf16[8,512,256]{2,1,0:T(8,128)(2,1)S(1)} %bitcast.61), channel_id=1, replica_groups=mesh['grp'=2,'fs'=16,'tp'=8] {'tp'}, dimensions={0} | all-to-all | bytes 4194304 | tf_op jit(solution)/shard_map/all_to_all | solution.py:39
  154.2 0.3 convert_reduce_fusion.1
  154.5 0.6 copy-done.2
  155.1 0.1 add_convert_fusion
  155.2 1.6 broadcast_in_dim.22
  156.7 4.7 %all-to-all-start.3 = ((bf16[8,4,128,256]{3,2,1,0:T(8,128)(2,1)}), bf16[8,4,128,256]{3,2,1,0:T(8,128)(2,1)S(1)}, u32[]{:S(2)}, u32[]{:S(2)}) async-start(bf16[8,4,128,256]{3,2,1,0:T(8,128)(2,1)} %broadcast_in_dim.22), calls=%async_computation.3 | async-start | bytes 4194304 | tf_op jit(solution)/shard_map/all_to_all | solution.py:15
  161.4 0.0 all-gather.5.cloned.1.call-start
  161.4 0.0 copy-done.3
  161.4 0.0 copy-done.4
  161.5 0.8 pad_maximum_fusion
  162.2 0.1 all-gather.5.cloned.1.call-update
  162.3 25.5 %all-to-all-done.3 = bf16[8,4,128,256]{3,2,1,0:T(8,128)(2,1)S(1)} async-done(((bf16[8,4,128,256]{3,2,1,0:T(8,128)(2,1)}), bf16[8,4,128,256]{3,2,1,0:T(8,128)(2,1)S(1)}, u32[]{:S(2)}, u32[]{:S(2)}) %all-to-all-start.3) | async-done | bytes 2097184 | tf_op jit(solution)/shard_map/all_to_all | solution.py:15
  187.7 0.0 copy-done.5
  187.7 2.1 stack.2
  189.8 8.1 %all-to-all-start.4 = ((bf16[16,704,128]{2,1,0:T(8,128)(2,1)}), bf16[16,704,128]{2,1,0:T(8,128)(2,1)}, u32[]{:S(2)}, u32[]{:S(2)}) async-start(bf16[16,704,128]{2,1,0:T(8,128)(2,1)} %stack.2), calls=%async_computation.4 | async-start | bytes 5767168 | tf_op jit(solution)/shard_map/all_to_all | solution.py:108
  198.0 0.5 convert_bitcast_fusion
  198.5 2.4 copy.29
  200.9 4.0 copy.38
  204.9 0.5 fusion.1
  205.4 168.4 %all-gather.5.cloned.1.call-done = bf16[2048,1408]{0,1:T(8,128)(2,1)} async-done(((bf16[128,1408]{0,1:T(8,128)(2,1)}), bf16[2048,1408]{0,1:T(8,128)(2,1)}) %all-gather.5.cloned.1.call-update) | async-done | bytes 5767184 | tf_op jit(solution)/shard_map/all_gather | solution.py:24
  373.8 0.0 copy-done.11
  373.8 6.0 %fusion.6 = f32[512,704]{0,1:T(8,128)} fusion(bf16[2048,1408]{0,1:T(8,128)(2,1)} %all-gather.5.cloned.1.call-done, f32[512,2048]{1,0:T(8,128)} %bitcast.64, f32[2048]{0:T(1024)S(1)} %copy-done.11, f32[512]{0:T(512)S(1)} %rsqrt_bitcast_fusion.1), kind=kOutput, calls=%fused_computation.16 | convolution fusion | flops 1479540736 | bytes 8529920 | tf_op jit(solution)/shard_map/dot_general | solution.py:102
  379.8 0.0 all-to-all-done.4
  379.8 7.8 %convolution_convert_fusion.1 = bf16[512,2048]{1,0:T(8,128)(2,1)S(1)} fusion(bf16[2048,1408]{0,1:T(8,128)(2,1)} %all-gather.5.cloned.1.call-done, f32[512,704]{0,1:T(8,128)} %fusion.6, f32[512,2048]{1,0:T(8,128)} %bitcast.65, f32[2048]{0:T(1024)S(1)} %copy-done.11, f32[512]{0:T(512)S(1)} %rsqrt_bitcast_fusion.1, bf16[16,704,128]{2,1,0:T(8,128)(2,1)} %all-to-all-done.4), kind=kOutput, calls=%fused_computation.11 | convolution fusion | flops 2959147008 | bytes 13510656 | tf_op jit(solution)/shard_map/dot_general | solution.py:105
  387.6 0.1 copy.45
  387.8 0.0 copy-start.1
  387.8 38.3 %all_to_all.37 = bf16[8,512,256]{2,1,0:T(8,128)(2,1)S(1)} all-to-all(bf16[8,512,256]{2,1,0:T(8,128)(2,1)S(1)} %bitcast.62), channel_id=1, replica_groups=mesh['grp'=2,'fs'=16,'tp'=8] {'tp'}, dimensions={0} | all-to-all | bytes 4194304 | tf_op jit(solution)/shard_map/all_to_all | solution.py:39
  426.1 0.3 convert_reduce_fusion
  426.4 0.1 multiply_reduce_fusion
  426.5 0.6 broadcast_in_dim.24
  427.2 4.3 all-to-all-start.6
  431.5 0.8 dynamic_slice.7
  432.2 4.0 all-to-all-done.6
  436.2 0.8 multiply_convert_fusion.2
  437.1 0.0 copy-done.1
  (15 shorter events, 0.1 us)
Async XLA Ops:
  6.5 27.5 %copy-start = (f32[3,1024]{1,0:T(4,128)S(1)}, f32[3,1024]{1,0:T(4,128)}, u32[]{:S(2)}) copy-start(f32[3,1024]{1,0:T(4,128)} %param.17) | copy-start | bytes 36868
  9.1 24.1 %copy-start.7 = (bf16[128,128]{1,0:T(8,128)(2,1)S(1)}, bf16[128,128]{1,0:T(8,128)(2,1)}, u32[]{:S(2)}) copy-start(bf16[128,128]{1,0:T(8,128)(2,1)} %param.16) | copy-start | bytes 98308
  9.1 24.1 %copy-start.8 = (bf16[128,128]{1,0:T(8,128)(2,1)S(1)}, bf16[128,128]{1,0:T(8,128)(2,1)}, u32[]{:S(2)}) copy-start(bf16[128,128]{1,0:T(8,128)(2,1)} %param.15) | copy-start | bytes 98308
  9.1 24.1 %copy-start.9 = (bf16[128,128]{1,0:T(8,128)(2,1)S(1)}, bf16[128,128]{1,0:T(8,128)(2,1)}, u32[]{:S(2)}) copy-start(bf16[128,128]{1,0:T(8,128)(2,1)} %param.14) | copy-start | bytes 98308
  9.1 24.8 %copy-start.6 = (bf16[128,128]{1,0:T(8,128)(2,1)S(1)}, bf16[128,128]{1,0:T(8,128)(2,1)}, u32[]{:S(2)}) copy-start(bf16[128,128]{1,0:T(8,128)(2,1)} %param.18) | copy-start | bytes 98308
  9.1 50.4 %all-to-all-start = ((bf16[8,4,128,256]{3,2,1,0:T(8,128)(2,1)}), bf16[8,4,128,256]{3,2,1,0:T(8,128)(2,1)S(1)}, u32[]{:S(2)}, u32[]{:S(2)}) async-start(bf16[8,4,128,256]{3,2,1,0:T(8,128)(2,1)} %broadcast_in_dim.20), calls=%async_computation | async-start | bytes 4194304 | tf_op jit(solution)/shard_map/all_to_all | solution.py:15
  33.2 73.9 %all-gather.3.cloned.1.call-start = ((), (), s32[]{:S(2)}) async-start(), calls=%async_computation.7 | async-start | bytes 1671168 | tf_op jit(solution)/shard_map/all_gather | solution.py:24
  60.4 50.3 %all-to-all-start.1 = ((bf16[16,128,128]{1,2,0:T(8,128)(2,1)}), bf16[16,128,128]{1,2,0:T(8,128)(2,1)S(1)}, u32[]{:S(2)}, u32[]{:S(2)}) async-start(bf16[16,128,128]{1,2,0:T(8,128)(2,1)} %broadcast_in_dim.21), calls=%async_computation.1 | async-start | bytes 1048576 | tf_op jit(solution)/shard_map/all_to_all | solution.py:15
  71.0 0.7 copy-start.10
  154.2 1.0 copy-start.2
  156.7 4.7 %copy-start.3 = (bf16[128,704]{0,1:T(8,128)(2,1)S(1)}, bf16[128,704]{0,1:T(8,128)(2,1)}, u32[]{:S(2)}) copy-start(bf16[128,704]{0,1:T(8,128)(2,1)} %param.21) | copy-start | bytes 540676
  156.7 4.7 %copy-start.4 = (bf16[128,704]{0,1:T(8,128)(2,1)S(1)}, bf16[128,704]{0,1:T(8,128)(2,1)}, u32[]{:S(2)}) copy-start(bf16[128,704]{0,1:T(8,128)(2,1)} %param.20) | copy-start | bytes 540676
  156.7 31.0 %copy-start.5 = (bf16[704,128]{1,0:T(8,128)(2,1)S(1)}, bf16[704,128]{1,0:T(8,128)(2,1)}, u32[]{:S(2)}) copy-start(bf16[704,128]{1,0:T(8,128)(2,1)} %param.22) | copy-start | bytes 540676
  156.7 31.0 %all-to-all-start.3 = ((bf16[8,4,128,256]{3,2,1,0:T(8,128)(2,1)}), bf16[8,4,128,256]{3,2,1,0:T(8,128)(2,1)S(1)}, u32[]{:S(2)}, u32[]{:S(2)}) async-start(bf16[8,4,128,256]{3,2,1,0:T(8,128)(2,1)} %broadcast_in_dim.22), calls=%async_computation.3 | async-start | bytes 4194304 | tf_op jit(solution)/shard_map/all_to_all | solution.py:15
  161.4 212.4 %all-gather.5.cloned.1.call-start = ((), (), s32[]{:S(2)}) async-start(), calls=%async_computation.8 | async-start | bytes 6127616 | tf_op jit(solution)/shard_map/all_gather | solution.py:24
  189.8 189.9 %all-to-all-start.4 = ((bf16[16,704,128]{2,1,0:T(8,128)(2,1)}), bf16[16,704,128]{2,1,0:T(8,128)(2,1)}, u32[]{:S(2)}, u32[]{:S(2)}) async-start(bf16[16,704,128]{2,1,0:T(8,128)(2,1)} %stack.2), calls=%async_computation.4 | async-start | bytes 5767168 | tf_op jit(solution)/shard_map/all_to_all | solution.py:108
  204.9 168.9 %copy-start.11 = (f32[2048]{0:T(1024)S(1)}, f32[2048]{0:T(1024)}, u32[]{:S(2)}) copy-start(f32[2048]{0:T(1024)} %param.19) | copy-start | bytes 24580
  387.8 49.3 %copy-start.1 = (f32[3,1024]{1,0:T(4,128)S(1)}, f32[3,1024]{1,0:T(4,128)}, u32[]{:S(2)}) copy-start(f32[3,1024]{1,0:T(4,128)} %param.17) | copy-start | bytes 36868
  427.2 9.0 %all-to-all-start.6 = ((f32[8,1,512]{2,1,0:T(1,128)}), f32[8,1,512]{2,1,0:T(1,128)S(1)}, u32[]{:S(2)}, u32[]{:S(2)}) async-start(f32[8,1,512]{2,1,0:T(1,128)} %broadcast_in_dim.24), calls=%async_computation.6 | async-start | bytes 32768 | tf_op jit(solution)/shard_map/all_to_all | solution.py:15
Sparse Core Ops, SparseCore 0:
  35.8 71.2 all-gather.2
  164.0 209.8 all-gather.4
